TPU v7x, 32 devices: a whole 2x2x4 slice. The times are simulated.
32 devices in a mesh: sp: 16 (over z, y, x), tp: 2 (over core).
Axes of the slice: x: 2, y: 2, z: 4, core: 2. Of those that a mesh axis runs over, the one named last changes fastest.
Arguments:
- tokens: bfloat16 [4096, 2048], P('sp', 'tp'), may hold values from -12 to 12
- norm_gain: float32 [2048], replicated, may hold values from 0.1 to 1.9
- window_query: bfloat16 [2048, 1024], P(None, 'tp'), may hold values from -2 to 2
- window_key: bfloat16 [2048, 512], P(None, 'tp'), may hold values from -2 to 2
- window_value: bfloat16 [2048, 512], P(None, 'tp'), may hold values from -0.125 to 0.125
- window_gate: bfloat16 [2048, 1024], P(None, 'tp'), may hold values from -0.125 to 0.125
- window_sink: float32 [16], P('tp'), may hold values from 2 to 6
- pair_query: bfloat16 [2048, 1024], P(None, 'tp'), may hold values from -2 to 2
- pair_key: bfloat16 [2048, 1024], P(None, 'tp'), may hold values from -2 to 2
- pair_value: bfloat16 [2048, 1024], P(None, 'tp'), may hold values from -0.125 to 0.125
- pair_gate: bfloat16 [2048, 1024], P(None, 'tp'), may hold values from -0.125 to 0.125
- map_lambda: float32 [8], P('tp'), may hold values from 0.3 to 0.8
- head_gain: float32 [128], replicated, may hold values from 0.1 to 1.9
- window_out: bfloat16 [1024, 2048], P('tp'), may hold values from -0.125 to 0.125
- pair_out: bfloat16 [1024, 2048], P('tp'), may hold values from -0.125 to 0.125
Outputs:
- mixed: bfloat16 [4096, 2048], P(('sp', 'tp'))
All inputs are finite; a program needn't handle non-finite values.
Results may differ from a plain program's by a relative error of at most 0.018.
Values may be sent and summed in bfloat16 or wider, within the bound.
A program may use at most 128 MiB of HBM per device.

v0:
```python
import jax
import jax.numpy as jnp
from jax import lax
from jax.sharding import PartitionSpec as P

HD = 64
WINDOW = 128


norm_eps = 1e-06
head_scale = 0.8


def swapped(value, axis, stride):
    mask = 2**stride
    pairs = [(source, source ^ mask) for source in range(lax.axis_size(axis))]
    return lax.ppermute(value, axis, pairs)


def shifted(value, axis, steps):
    count = lax.axis_size(axis)
    initial, last = (max(0, -steps), min(count, count - steps))
    return lax.ppermute(value, axis, [(source, source + steps) for source in range(initial, last)])


def row_norm(values, gain_vec):
    squares = jnp.mean(values * values, axis=-1, keepdims=True)
    return values * lax.rsqrt(squares + norm_eps) * gain_vec


def key_block(row_count, shard_rows):
    shards = row_count // shard_rows
    chosen = 1
    for factor in range(1, shards + 1):
        if shards % factor == 0 and factor * shard_rows <= 1024:
            chosen = factor
    return chosen * shard_rows


def fold_rows(current, key_piece, value_piece, queries, positions, shard_rows):
    row_count = key_piece.shape[0]
    block_rows = key_block(row_count, shard_rows)
    query_rows = queries.shape[0]
    heads = queries.shape[1] // (2 * HD)
    shaped = queries.reshape(query_rows, heads, 2, HD)
    needed = jnp.clip(positions[query_rows - 1] // block_rows + 1, 0, row_count // block_rows)

    def one_step(turn_index, carried):
        running_top, running_total, running_acc = carried
        begin = turn_index * block_rows
        key_rows = lax.dynamic_slice_in_dim(key_piece, begin, block_rows, 0).reshape(
            block_rows, heads, 2, HD
        )
        value_rows = lax.dynamic_slice_in_dim(value_piece, begin, block_rows, 0).reshape(
            block_rows, heads, 2 * HD
        )
        key_pos = begin + jnp.arange(block_rows, dtype=jnp.int32)
        scores = jnp.einsum(
            "ihcd,jhcd->hcij", shaped, key_rows, preferred_element_type=jnp.float32
        ) * HD ** (-0.5)
        causal = positions[:, None] >= key_pos[None, :]
        masked = jnp.where(causal, scores, -jnp.inf)
        new_top = jnp.maximum(running_top, jnp.max(masked, axis=-1))
        factor = jnp.exp(running_top - new_top)
        weights = jnp.where(causal, jnp.exp(masked - new_top[..., None]), 0.0)
        new_total = running_total * factor + jnp.sum(weights, axis=-1)
        new_acc = running_acc * factor[..., None] + jnp.einsum(
            "hcij,jhe->hcie",
            weights.astype(jnp.bfloat16),
            value_rows,
            preferred_element_type=jnp.float32,
        )
        return (new_top, new_total, new_acc)

    return lax.fori_loop(0, needed, one_step, current)


def finish(final, gate_rows, map_lambda, head_gain):
    final_top, final_total, final_acc = final
    row_count = gate_rows.shape[0]
    heads = gate_rows.shape[1] // (2 * HD)
    per_map = final_acc / final_total[..., None]
    differ = per_map[:, 0] - map_lambda[:, None, None] * per_map[:, 1]
    head_out = jnp.transpose(row_norm(differ, head_gain) * head_scale, (1, 0, 2))
    gate_act = jax.nn.silu(gate_rows.astype(jnp.float32).reshape(row_count, heads, 2 * HD))
    return (head_out * gate_act).reshape(row_count, heads * 2 * HD).astype(jnp.bfloat16)


def per_device(
    tokens,
    norm_gain,
    window_query,
    window_key,
    window_value,
    window_gate,
    window_sink,
    pair_query,
    pair_key,
    pair_value,
    pair_gate,
    map_lambda,
    head_gain,
    window_out,
    pair_out,
):
    tok_rows = tokens.shape[0]
    gathered = lax.all_gather(tokens, "tp", axis=1, tiled=True)
    normed = row_norm(gathered.astype(jnp.float32), norm_gain).astype(jnp.bfloat16)

    def project(weight):
        return jnp.dot(normed, weight, preferred_element_type=jnp.float32).astype(jnp.bfloat16)

    slide_query = project(window_query)
    slide_key = project(window_key)
    slide_value = project(window_value)
    slide_gate = project(window_gate)
    paired_query = project(pair_query)
    paired_key = project(pair_key)
    paired_value = project(pair_value)
    paired_gate = project(pair_gate)
    scale = HD ** (-0.5)
    kv_heads = slide_key.shape[1] // HD
    group_size = slide_query.shape[1] // slide_key.shape[1]
    pair_heads = paired_query.shape[1] // (2 * HD)
    offset = lax.axis_index("sp") * tok_rows
    query_pos = offset + jnp.arange(tok_rows, dtype=jnp.int32)
    half_rows = tok_rows // 2
    travel = jnp.stack([paired_query[half_rows:], paired_gate[half_rows:]])
    for bit in range(lax.axis_size("sp").bit_length() - 1):
        travel = swapped(travel, "sp", bit)
    mirror_offset = (lax.axis_size("sp") - 1 - lax.axis_index("sp")) * tok_rows
    groups = (
        (paired_query[:half_rows], query_pos[:half_rows]),
        (travel[0], mirror_offset + half_rows + jnp.arange(half_rows, dtype=jnp.int32)),
    )
    gates = (paired_gate[:half_rows], travel[1])
    start_states = tuple(
        (
            (
                jnp.full((pair_heads, 2, member[0].shape[0]), -1e30, jnp.float32),
                jnp.zeros((pair_heads, 2, member[0].shape[0]), jnp.float32),
                jnp.zeros((pair_heads, 2, member[0].shape[0], 2 * HD), jnp.float32),
            )
            for member in groups
        )
    )
    tail_keys, tail_values = shifted(
        (slide_key[tok_rows - WINDOW :], slide_value[tok_rows - WINDOW :]), "sp", 1
    )
    key_piece = lax.all_gather(paired_key, "sp", axis=0, tiled=True)
    value_piece = lax.all_gather(paired_value, "sp", axis=0, tiled=True)
    final_states = tuple(
        (
            fold_rows(current, key_piece, value_piece, member[0], member[1], tok_rows)
            for current, member in zip(start_states, groups)
        )
    )
    band_keys = jnp.concatenate([tail_keys, slide_key], axis=0).reshape(
        WINDOW + tok_rows, kv_heads, HD
    )
    band_values = jnp.concatenate([tail_values, slide_value], axis=0).reshape(
        WINDOW + tok_rows, kv_heads, HD
    )
    band_pos = offset - WINDOW + jnp.arange(WINDOW + tok_rows, dtype=jnp.int32)
    window_queries = slide_query.reshape(tok_rows, kv_heads, group_size, HD)
    scores = (
        jnp.einsum("ikgd,jkd->kgij", window_queries, band_keys, preferred_element_type=jnp.float32)
        * scale
    )
    distance = query_pos[:, None] - band_pos[None, :]
    valid = (distance >= 0) & (distance < WINDOW) & (band_pos[None, :] >= 0)
    masked = jnp.where(valid, scores, -jnp.inf)
    sink_logit = window_sink.reshape(kv_heads, group_size)[:, :, None, None]
    top = jnp.maximum(jnp.max(masked, axis=-1, keepdims=True), sink_logit)
    weights = jnp.where(valid, jnp.exp(masked - top), 0.0)
    probs = (
        weights / (jnp.sum(weights, axis=-1, keepdims=True) + jnp.exp(sink_logit - top))
    ).astype(jnp.bfloat16)
    slide_out = jnp.einsum("kgij,jkd->ikgd", probs, band_values, preferred_element_type=jnp.float32)
    slide_out = slide_out.reshape(tok_rows, kv_heads * group_size * HD)
    slide_mix = (slide_out * jax.nn.silu(slide_gate.astype(jnp.float32))).astype(jnp.bfloat16)
    mixes = tuple(
        (
            finish(final, gate_rows, map_lambda, head_gain)
            for final, gate_rows in zip(final_states, gates)
        )
    )
    returned = mixes[1]
    for bit in range(lax.axis_size("sp").bit_length() - 1):
        returned = swapped(returned, "sp", bit)
    paired_mix = jnp.concatenate([mixes[0], returned], axis=0)
    partial_sum = jnp.dot(slide_mix, window_out, preferred_element_type=jnp.float32)
    partial_sum = partial_sum + jnp.dot(paired_mix, pair_out, preferred_element_type=jnp.float32)
    return lax.psum_scatter(
        lax.optimization_barrier(partial_sum.astype(jnp.bfloat16))
        .astype(jnp.float32)
        .astype(jnp.bfloat16),
        "tp",
        scatter_dimension=0,
        tiled=True,
    )


def solution(mesh):
    in_specs = (
        P("sp", "tp"),
        P(),
        P(None, "tp"),
        P(None, "tp"),
        P(None, "tp"),
        P(None, "tp"),
        P("tp"),
        P(None, "tp"),
        P(None, "tp"),
        P(None, "tp"),
        P(None, "tp"),
        P("tp"),
        P(),
        P("tp", None),
        P("tp", None),
    )
    out_specs = P(("sp", "tp"), None)
    return jax.shard_map(
        per_device, mesh=mesh, in_specs=in_specs, out_specs=out_specs, check_vma=False
    )
```

profile of v0, /device:TPU:31, one launch (start us, length us, event | category | flops | bytes accessed | tf_op | source)
XLA Modules:
  0.0 269.0 jit_solution(7774299127174353839)
XLA Ops:
  7.3 12.3 %all-gather.4.cloned.1.call-done = bf16[256,2048]{1,0:T(8,128)(2,1)} async-done(((bf16[256,1024]{1,0:T(8,128)(2,1)}), bf16[256,2048]{1,0:T(8,128)(2,1)}) %all-gather.4.cloned.1.call-update) | async-done | bytes 1048592 | tf_op jit(solution)/shard_map/all_gather | solution.py:107
  19.6 1.6 fusion.29
  21.2 3.4 %convolution_convert_fusion.3 = bf16[256,512]{1,0:T(8,128)(2,1)} fusion(bf16[2048,512]{1,0:T(8,128)(2,1)} %param.27, bf16[256,2048]{1,0:T(8,128)(2,1)} %all-gather.4.cloned.1.call-done, f32[2048]{0:T(1024)} %param.20, f32[256]{0:T(256)S(1)} %add_rsqrt_fusion.2), kind=kOutput, calls=%fused_computation.52 | convolution fusion | flops 539099136 | bytes 3417088 | tf_op jit(solution)/shard_map/dot_general | solution.py:111
  24.7 3.1 %convolution_convert_fusion.1 = bf16[256,512]{1,0:T(8,128)(2,1)} fusion(bf16[2048,512]{1,0:T(8,128)(2,1)} %param.28, bf16[256,2048]{1,0:T(8,128)(2,1)S(1)} %copy-done.2, f32[2048]{0:T(1024)S(1)} %copy-done.24, f32[256]{0:T(256)S(1)} %add_rsqrt_fusion.2), kind=kOutput, calls=%fused_computation.50 | convolution fusion | flops 539099136 | bytes 3417088 | tf_op jit(solution)/shard_map/dot_general | solution.py:111
  35.1 2.5 convolution_convert_fusion
  42.6 4.3 %collective-permute-done.2 = bf16[2,128,512]{2,1,0:T(8,128)(2,1)S(1)} collective-permute-done((bf16[2,128,512]{2,1,0:T(8,128)(2,1)S(1)}, bf16[2,128,512]{2,1,0:T(8,128)(2,1)S(1)}, u32[]{:S(2)}, u32[]{:S(2)}) %collective-permute-start.2) | collective-permute-done | bytes 262176 | tf_op jit(solution)/shard_map/ppermute | solution.py:17
  48.6 4.5 %collective-permute-done.3 = bf16[2,128,512]{2,1,0:T(8,128)(2,1)} collective-permute-done((bf16[2,128,512]{2,1,0:T(8,128)(2,1)S(1)}, bf16[2,128,512]{2,1,0:T(8,128)(2,1)}, u32[]{:S(2)}, u32[]{:S(2)}) %collective-permute-start.3) | collective-permute-done | bytes 262176 | tf_op jit(solution)/shard_map/ppermute | solution.py:17
  60.6 7.6 %collective-permute-done.4 = bf16[2,128,512]{2,1,0:T(8,128)(2,1)} collective-permute-done((bf16[2,128,512]{2,1,0:T(8,128)(2,1)}, bf16[2,128,512]{2,1,0:T(8,128)(2,1)}, u32[]{:S(2)}, u32[]{:S(2)}) %collective-permute-start.4) | collective-permute-done | bytes 262176 | tf_op jit(solution)/shard_map/ppermute | solution.py:17
  68.2 2.3 fusion.26
  71.2 20.4 %collective-permute-done.5 = bf16[2,128,512]{2,1,0:T(8,128)(2,1)S(1)} collective-permute-done((bf16[2,128,512]{2,1,0:T(8,128)(2,1)}, bf16[2,128,512]{2,1,0:T(8,128)(2,1)S(1)}, u32[]{:S(2)}, u32[]{:S(2)}) %collective-permute-start.5) | collective-permute-done | bytes 262176 | tf_op jit(solution)/shard_map/ppermute | solution.py:17
  92.6 13.3 %all-gather.6.cloned.1.call-done = bf16[4096,512]{1,0:T(8,128)(2,1)} async-done(((bf16[256,512]{1,0:T(8,128)(2,1)}), bf16[4096,512]{1,0:T(8,128)(2,1)}) %all-gather.6.cloned.1.call-update) | async-done | bytes 4194320 | tf_op jit(solution)/shard_map/all_gather | solution.py:150
  105.9 6.4 %copy.44 = bf16[4096,512]{0,1:T(8,128)(2,1)} copy(bf16[4096,512]{1,0:T(8,128)(2,1)} %all-gather.6.cloned.1.call-done) | data formatting | bytes 8388608 | tf_op jit(solution)/shard_map/while | solution.py:75
  112.2 69.7 %all-gather.8.cloned.1.call-done = bf16[4096,512]{1,0:T(8,128)(2,1)} async-done(((bf16[256,512]{1,0:T(8,128)(2,1)}), bf16[4096,512]{1,0:T(8,128)(2,1)}) %all-gather.8.cloned.1.call-update) | async-done | bytes 4194320 | tf_op jit(solution)/shard_map/all_gather | solution.py:151
  182.0 6.5 %copy.45 = bf16[4096,512]{0,1:T(8,128)(2,1)} copy(bf16[4096,512]{1,0:T(8,128)(2,1)} %all-gather.8.cloned.1.call-done) | data formatting | bytes 8388608 | tf_op jit(solution)/shard_map/while | solution.py:75
  188.5 5.6 %while.30 = (s32[]{:T(128)}, f32[4,2,128]{2,1,0:T(2,128)S(1)}, f32[4,2,128]{2,1,0:T(2,128)S(1)}, f32[4,2,128,128]{3,2,1,0:T(8,128)S(1)}, s32[]{:T(128)}, /*index...) while((s32[]{:T(128)}, f32[4,2,128]{2,1,0:T(2,128)S(1)}, ...), condition=%wide.region_11.12_spmd.clone, body=%wide.region_8.11_spmd.clone.sunk | while | flops 416681088 | bytes 20653240 | solution.py:75
  188.5 1.7 constant_dynamic-slice_fusion.7
  192.6 1.5 fusion.109
  194.9 22.5 %while.29 = (s32[]{:T(128)}, f32[4,2,128]{2,1,0:T(2,128)S(1)}, f32[4,2,128]{2,1,0:T(2,128)S(1)}, f32[4,2,128,128]{3,2,1,0:T(8,128)S(1)}, s32[]{:T(128)}, /*index...) while((s32[]{:T(128)}, f32[4,2,128]{2,1,0:T(2,128)S(1)}, ...), condition=%wide.region_6.7_spmd, body=%wide.region_3.6_spmd.sunk | while | flops 416680960 | bytes 20654800 | solution.py:75
  195.2 1.7 constant_dynamic-slice_fusion.6
  199.2 1.5 fusion.102
  200.8 1.7 constant_dynamic-slice_fusion.6
  204.8 1.5 fusion.102
  206.3 1.7 constant_dynamic-slice_fusion.6
  211.9 1.7 constant_dynamic-slice_fusion.6
  220.8 1.9 fusion.45
  227.7 2.7 collective-permute-done.7
  231.6 3.8 %fusion.32 = f32[4,64,2,256]{3,1,2,0:T(8,128)} fusion(bf16[384,4,64,1]{0,2,3,1:T(8,128)(2,1)S(1)} %bitcast.228, f32[4,384,256,2]{2,1,3,0:T(8,128)} %get-tuple-element.224, f32[4,2,256]{2,1,0:T(2,128)S(1)} %exponential_add_fusion, f32[4,2,256]{2,1,0:T(2,128)S(1)} %copy-done.11, pred[256,384]{0,1:T(8,128)(4,1)S(1)} %copy-done.6), kind=kOutput, calls=%fused_computation.48 | convolution fusion | flops 105381888 | bytes 3981312 | tf_op jit(solution)/shard_map/kgij,jkd->ikgd/dot_general | solution.py:179
  235.5 2.1 copy.42
  237.6 4.5 %fusion.34 = f32[256,2048]{1,0:T(8,128)} fusion(bf16[512,2048]{1,0:T(8,128)(2,1)S(1)} %copy-done, f32[256,512]{1,0:T(8,128)} %copy.42, bf16[2048,512]{1,0:T(8,128)(2,1)} %param.24, bf16[256,2048]{1,0:T(8,128)(2,1)S(1)} %copy-done.3, f32[2048]{0:T(1024)S(1)} %copy-done.25, f32[256]{0:T(256)S(1)} %copy-done.17), kind=kOutput, calls=%fused_computation.61 | convolution fusion | flops 1076887552 | bytes 7873536 | tf_op jit(solution)/shard_map/dot_general | solution.py:192
  242.1 1.8 collective-permute-done.9
  243.9 3.9 %fusion.27 = bf16[256,2048]{1,0:T(8,128)(2,1)} fusion(f32[256,2048]{1,0:T(8,128)} %fusion.34, bf16[512,2048]{1,0:T(8,128)(2,1)} %param.33, bf16[128,512]{0,1:T(8,128)(2,1)S(1)} %collective-permute-done.9, bf16[128,512]{0,1:T(8,128)(2,1)S(1)} %bitcast.218), kind=kOutput, calls=%fused_computation.43 | convolution fusion | flops 538443776 | bytes 5505024 | tf_op jit(solution)/shard_map/dot_general | solution.py:193
  247.8 14.7 %reduce-scatter.2.cloned.1.call-done = bf16[128,2048]{1,0:T(8,128)(2,1)} async-done(((bf16[256,2048]{1,0:T(8,128)(2,1)}), bf16[128,2048]{1,0:T(8,128)(2,1)}) %reduce-scatter.2.cloned.1.call-update) | async-done | bytes 524304 | tf_op jit(solution)/shard_map/reduce_scatter | solution.py:194
  (164 shorter events, 43.5 us)
Async XLA Ops:
  6.5 231.0 %copy-start = (bf16[512,2048]{1,0:T(8,128)(2,1)S(1)}, bf16[512,2048]{1,0:T(8,128)(2,1)}, u32[]{:S(2)}) copy-start(bf16[512,2048]{1,0:T(8,128)(2,1)} %param.32) | copy-start | bytes 6291460
  6.5 18.1 %copy-start.24 = (f32[2048]{0:T(1024)S(1)}, f32[2048]{0:T(1024)}, u32[]{:S(2)}) copy-start(f32[2048]{0:T(1024)} %param.20) | copy-start | bytes 24580
  6.5 13.0 %all-gather.4.cloned.1.call-start = ((), (), s32[]{:S(2)}) async-start(), calls=%async_computation.1 | async-start | bytes 1572864 | tf_op jit(solution)/shard_map/all_gather | solution.py:107
  7.3 98.6 %all-gather.6.cloned.1.call-start = ((), (), s32[]{:S(2)}) async-start(), calls=%async_computation.2 | async-start | bytes 4456448 | tf_op jit(solution)/shard_map/all_gather | solution.py:150
  21.2 32.2 %copy-start.16 = (f32[256]{0:T(256)}, f32[256]{0:T(256)S(1)}, u32[]{:S(2)}) copy-start(f32[256]{0:T(256)S(1)} %add_rsqrt_fusion.2) | copy-start | bytes 3076
  24.6 10.2 %copy-start.19 = (f32[8]{0:T(128)S(1)}, f32[8]{0:T(128)}, u32[]{:S(2)}) copy-start(f32[8]{0:T(128)} %param.25) | copy-start | bytes 100
  24.6 157.3 %all-gather.8.cloned.1.call-start = ((), (), s32[]{:S(2)}) async-start(), calls=%async_computation.3 | async-start | bytes 4456448 | tf_op jit(solution)/shard_map/all_gather | solution.py:151
  27.8 234.7 %reduce-scatter.2.cloned.1.call-start = ((), (), s32[]{:S(2)}) async-start(), calls=%async_computation.4 | async-start | bytes 1572864 | tf_op jit(solution)/shard_map/reduce_scatter | solution.py:194
  34.9 35.7 %copy-start.12 = (f32[4,2]{1,0:T(4,128)}, f32[4,2]{1,0:T(4,128)S(1)}, u32[]{:S(2)}) copy-start(f32[4,2]{1,0:T(4,128)S(1)} %max.31) | copy-start | bytes 100
  35.1 33.1 %copy-start.4 = (pred[256,384]{0,1:T(8,128)(4,1)}, pred[256,384]{0,1:T(8,128)(4,1)S(1)}, u32[]{:S(2)}) copy-start(pred[256,384]{0,1:T(8,128)(4,1)S(1)} %fusion.36) | copy-start | bytes 294916
  38.4 8.8 %copy-start.21 = (bf16[2048,512]{1,0:T(8,128)(2,1)S(1)}, bf16[2048,512]{1,0:T(8,128)(2,1)}, u32[]{:S(2)}) copy-start(bf16[2048,512]{1,0:T(8,128)(2,1)} %param.21) | copy-start | bytes 6291460
  39.2 7.7 %collective-permute-start.2 = (bf16[2,128,512]{2,1,0:T(8,128)(2,1)S(1)}, bf16[2,128,512]{2,1,0:T(8,128)(2,1)S(1)}, u32[]{:S(2)}, u32[]{:S(2)}) collective-permute-start(bf16[2,128,512]{2,1,0:T(8,128)(2,1)S(1)} %pad_maximum_fusion), channel_id=1, source_target_pairs={{0,2},{2,0},{4,6},{6,4},{8,10},{10,8},{12,14},{14,12},{16,18},{18,... | collective-permute-start | bytes 786440 | tf_op jit(solution)/shard_map/ppermute | solution.py:17
  40.7 12.7 %copy-start.23 = (bf16[2048,256]{1,0:T(8,128)(2,1)S(1)}, bf16[2048,256]{1,0:T(8,128)(2,1)}, u32[]{:S(2)}) copy-start(bf16[2048,256]{1,0:T(8,128)(2,1)} %param.23) | copy-start | bytes 3145732
  41.3 18.2 %collective-permute-start.1 = (bf16[128,256]{1,0:T(8,128)(2,1)}, bf16[128,256]{1,0:T(8,128)(2,1)}, u32[]{:S(2)}, u32[]{:S(2)}) collective-permute-start(bf16[128,256]{1,0:T(8,128)(2,1)} %slice.62), channel_id=1, source_target_pairs={{0,2},{2,4},{4,6},{6,8},{8,10},{10,12},{12,14},{14,16},{16,18},{18... | collective-permute-start | bytes 196616 | tf_op jit(solution)/shard_map/ppermute | solution.py:23
  46.9 6.2 %collective-permute-start.3 = (bf16[2,128,512]{2,1,0:T(8,128)(2,1)S(1)}, bf16[2,128,512]{2,1,0:T(8,128)(2,1)}, u32[]{:S(2)}, u32[]{:S(2)}) collective-permute-start(bf16[2,128,512]{2,1,0:T(8,128)(2,1)S(1)} %collective-permute-done.2), channel_id=1, source_target_pairs={{0,4},{2,6},{4,0},{6,2},{8,12},{10,14},{12,8},{14,10},{16,20},{18,... | collective-permute-start | bytes 786440 | tf_op jit(solution)/shard_map/ppermute | solution.py:17
  53.1 15.1 %collective-permute-start.4 = (bf16[2,128,512]{2,1,0:T(8,128)(2,1)}, bf16[2,128,512]{2,1,0:T(8,128)(2,1)}, u32[]{:S(2)}, u32[]{:S(2)}) collective-permute-start(bf16[2,128,512]{2,1,0:T(8,128)(2,1)} %collective-permute-done.3), channel_id=1, source_target_pairs={{0,8},{2,10},{4,12},{6,14},{8,0},{10,2},{12,4},{14,6},{16,24},{18,... | collective-permute-start | bytes 786440 | tf_op jit(solution)/shard_map/ppermute | solution.py:17
  58.3 166.4 %collective-permute-start = (bf16[128,256]{1,0:T(8,128)(2,1)}, bf16[128,256]{1,0:T(8,128)(2,1)}, u32[]{:S(2)}, u32[]{:S(2)}) collective-permute-start(bf16[128,256]{1,0:T(8,128)(2,1)} %slice.61), channel_id=1, source_target_pairs={{0,2},{2,4},{4,6},{6,8},{8,10},{10,12},{12,14},{14,16},{16,18},{18... | collective-permute-start | bytes 196616 | tf_op jit(solution)/shard_map/ppermute | solution.py:23
  68.2 23.3 %collective-permute-start.5 = (bf16[2,128,512]{2,1,0:T(8,128)(2,1)}, bf16[2,128,512]{2,1,0:T(8,128)(2,1)S(1)}, u32[]{:S(2)}, u32[]{:S(2)}) collective-permute-start(bf16[2,128,512]{2,1,0:T(8,128)(2,1)} %collective-permute-done.4), channel_id=1, source_target_pairs={{0,16},{2,18},{4,20},{6,22},{8,24},{10,26},{12,28},{14,30},{16,0},... | collective-permute-start | bytes 786440 | tf_op jit(solution)/shard_map/ppermute | solution.py:17
  217.5 6.3 %copy-start.5 = (pred[256,384]{0,1:T(8,128)(4,1)S(1)}, pred[256,384]{0,1:T(8,128)(4,1)}, u32[]{:S(2)}) copy-start(pred[256,384]{0,1:T(8,128)(4,1)} %copy-done.4) | copy-start | bytes 294916
  217.5 6.3 %copy-start.10 = (f32[4,2,256]{2,1,0:T(2,128)S(1)}, f32[4,2,256]{2,1,0:T(2,128)}, u32[]{:S(2)}) copy-start(f32[4,2,256]{2,1,0:T(2,128)} %broadcast_maximum_fusion) | copy-start | bytes 24580
  218.5 5.3 %copy-start.1 = (f32[4,384,256,2]{2,1,3,0:T(8,128)S(1)}, f32[4,384,256,2]{2,1,3,0:T(8,128)}, u32[]{:S(2)}) copy-start(f32[4,384,256,2]{2,1,3,0:T(8,128)} %get-tuple-element.224) | copy-start | bytes 9437188
  220.7 6.9 %copy-start.13 = (f32[4,2]{1,0:T(4,128)S(1)}, f32[4,2]{1,0:T(4,128)}, u32[]{:S(2)}) copy-start(f32[4,2]{1,0:T(4,128)} %copy-done.12) | copy-start | bytes 100
  220.8 10.9 %copy-start.6 = (pred[256,384]{0,1:T(8,128)(4,1)S(1)}, pred[256,384]{0,1:T(8,128)(4,1)}, u32[]{:S(2)}) copy-start(pred[256,384]{0,1:T(8,128)(4,1)} %copy-done.4) | copy-start | bytes 294916
  220.8 10.8 %copy-start.11 = (f32[4,2,256]{2,1,0:T(2,128)S(1)}, f32[4,2,256]{2,1,0:T(2,128)}, u32[]{:S(2)}) copy-start(f32[4,2,256]{2,1,0:T(2,128)} %broadcast_maximum_fusion) | copy-start | bytes 24580
  222.7 3.8 %collective-permute-start.6 = (bf16[128,512]{0,1:T(8,128)(2,1)S(1)}, bf16[128,512]{0,1:T(8,128)(2,1)S(1)}, u32[]{:S(2)}, u32[]{:S(2)}) collective-permute-start(bf16[128,512]{0,1:T(8,128)(2,1)S(1)} %bitcast.229), channel_id=1, source_target_pairs={{0,2},{2,0},{4,6},{6,4},{8,10},{10,8},{12,14},{14,12},{16,18},{18,... | collective-permute-start | bytes 393224 | tf_op jit(solution)/shard_map/ppermute | solution.py:17
  226.5 3.9 %collective-permute-start.7 = (bf16[128,512]{0,1:T(8,128)(2,1)S(1)}, bf16[128,512]{0,1:T(8,128)(2,1)}, u32[]{:S(2)}, u32[]{:S(2)}) collective-permute-start(bf16[128,512]{0,1:T(8,128)(2,1)S(1)} %collective-permute-done.6), channel_id=1, source_target_pairs={{0,4},{2,6},{4,0},{6,2},{8,12},{10,14},{12,8},{14,10},{16,20},{18,... | collective-permute-start | bytes 393224 | tf_op jit(solution)/shard_map/ppermute | solution.py:17
  230.4 7.1 %collective-permute-start.8 = (bf16[128,512]{0,1:T(8,128)(2,1)}, bf16[128,512]{0,1:T(8,128)(2,1)}, u32[]{:S(2)}, u32[]{:S(2)}) collective-permute-start(bf16[128,512]{0,1:T(8,128)(2,1)} %collective-permute-done.7), channel_id=1, source_target_pairs={{0,8},{2,10},{4,12},{6,14},{8,0},{10,2},{12,4},{14,6},{16,24},{18,... | collective-permute-start | bytes 393224 | tf_op jit(solution)/shard_map/ppermute | solution.py:17
  231.6 5.9 %copy-start.3 = (bf16[256,2048]{1,0:T(8,128)(2,1)S(1)}, bf16[256,2048]{1,0:T(8,128)(2,1)}, u32[]{:S(2)}) copy-start(bf16[256,2048]{1,0:T(8,128)(2,1)} %all-gather.4.cloned.1.call-done) | copy-start | bytes 3145732
  231.6 6.0 %copy-start.17 = (f32[256]{0:T(256)S(1)}, f32[256]{0:T(256)}, u32[]{:S(2)}) copy-start(f32[256]{0:T(256)} %copy-done.16) | copy-start | bytes 3076
  231.6 6.0 %copy-start.25 = (f32[2048]{0:T(1024)S(1)}, f32[2048]{0:T(1024)}, u32[]{:S(2)}) copy-start(f32[2048]{0:T(1024)} %param.20) | copy-start | bytes 24580
  237.5 6.3 %copy-start.7 = (bf16[128,4,128]{0,2,1:T(8,128)(2,1)S(1)}, bf16[128,4,128]{0,2,1:T(8,128)(2,1)}, u32[]{:S(2)}) copy-start(bf16[128,4,128]{0,2,1:T(8,128)(2,1)} %get-tuple-element.221) | copy-start | bytes 393220
  237.5 6.3 %collective-permute-start.9 = (bf16[128,512]{0,1:T(8,128)(2,1)}, bf16[128,512]{0,1:T(8,128)(2,1)S(1)}, u32[]{:S(2)}, u32[]{:S(2)}) collective-permute-start(bf16[128,512]{0,1:T(8,128)(2,1)} %collective-permute-done.8), channel_id=1, source_target_pairs={{0,16},{2,18},{4,20},{6,22},{8,24},{10,26},{12,28},{14,30},{16,0},... | collective-permute-start | bytes 393224 | tf_op jit(solution)/shard_map/ppermute | solution.py:17
  (11 other events, 27.9 us)
Sparse Core Ops, SparseCore 0:
  8.9 10.6 all-gather.3
  24.8 81.0 all-gather.5
  108.6 73.2 all-gather.7
  248.0 14.4 reduce-scatter.1
where the time goes:
time: 271 us; the launch traced here: 269 us
  waiting for transfers between devices  153 us (56%)
  matrix products  40.2 us (15%)
  local copies, waits for them, and re-layouts  33.7 us (12%)
  between operations  18.7 us (7%)
  other arithmetic  16.1 us (6%)
  starting transfers between devices  7.09 us (3%)
    all_gather x1, waiting for transfers between devices, per_device(): value_piece = lax.all_gather(paired_value, 'sp', axis=0, tiled=True)  69.7 us
    ppermute x8, waiting for transfers between devices, swapped(): return lax.ppermute(value, axis, pairs)  41.9 us
    reduce_scatter x1, waiting for transfers between devices, per_device(): lax.psum_scatter(lax.optimization_barrier(partial_sum.astype(jnp.bfloat16...  14.7 us
    while x6, local copies, waits for them, and re-layouts, fold_rows(): return lax.fori_loop(0, needed, one_step, current)  14.6 us
    all_gather x1, waiting for transfers between devices, per_device(): key_piece = lax.all_gather(paired_key, 'sp', axis=0, tiled=True)  13.3 us
    dot_general x7, matrix products, project(): jnp.dot(normed, weight, preferred_element_type=jnp.float32)  12.8 us
    all_gather x1, waiting for transfers between devices, per_device(): gathered = lax.all_gather(tokens, 'tp', axis=1, tiled=True)  12.3 us
    dynamic_slice x5, local copies, waits for them, and re-layouts, one_step(): lax.dynamic_slice_in_dim(value_piece, begin, block_rows, 0)  8.61 us
  transfers between devices with their start and end apart: 14, of which 11 were waited for; matrix products, arithmetic and copies ran while one was open for 30% of the time, Pallas kernels for 0%

commit v1 on v0

v1 whole, which is shorter than its diff:
```python
import functools
import math

import jax
import jax.numpy as jnp
from jax import lax
from jax.experimental import pallas as pl
from jax.experimental.pallas import tpu as pltpu
from jax.sharding import PartitionSpec as P

HD = 64
WINDOW = 128

norm_eps = 1e-06
head_scale = 0.8

MESH = pl.DeviceIdType.MESH
F32 = jnp.float32
BF16 = jnp.bfloat16


def dot_nt(a, b):
    return lax.dot_general(a, b, (((1,), (1,)), ((), ())), preferred_element_type=F32)


def dot_tn(a, b):
    return lax.dot_general(a, b, (((0,), (0,)), ((), ())), preferred_element_type=F32)


def silu(v):
    return v / (1.0 + jnp.exp(-v))


def kernel(
    S,
    T,
    tokens,
    norm_gain,
    wq_h,
    wk_h,
    wv_h,
    wg_h,
    sink,
    pq_h,
    pk_h,
    pv_h,
    pg_h,
    lam,
    head_gain,
    wo_h,
    po_h,
    out,
    wq,
    wk,
    wv,
    wg,
    pq,
    pk,
    pv,
    pg,
    wo,
    po,
    tok_buf,
    normed,
    band_k,
    band_v,
    sq_buf,
    sg_buf,
    pg_buf,
    slide_mix,
    paired_mix,
    kv_send,
    q_send,
    kv_all,
    q_all,
    q2_buf,
    m_buf,
    l_buf,
    acc_buf,
    ret_send,
    ret_all,
    part,
    part_bf,
    rs_buf,
    w_sem,
    tok_s,
    tok_r,
    kv1_s,
    kv2_s,
    kv_r,
    q_s,
    q_r,
    tail_s,
    tail_r,
    ret_s,
    ret_r,
    rs_s,
    rs_r,
):
    R = tokens.shape[0]
    Dl = tokens.shape[1]
    D = Dl * T
    G = kv_send.shape[0]
    M = S // G
    C = kv_send.shape[3]
    Hg = C // (2 * HD)
    s = lax.axis_index("sp")
    t = lax.axis_index("tp")
    g = s // M
    m = lax.rem(s, M)

    pairs = [(pk_h, pk), (pv_h, pv), (pq_h, pq), (wk_h, wk), (wv_h, wv), (wq_h, wq), (wg_h, wg), (pg_h, pg), (wo_h, wo), (po_h, po)]
    loads = [pltpu.make_async_copy(a, b, w_sem.at[i]) for i, (a, b) in enumerate(pairs)]
    for cp in loads:
        cp.start()

    barrier = pltpu.get_barrier_semaphore()
    for dt in range(1, T):
        pl.semaphore_signal(barrier, inc=1, device_id={"tp": lax.rem(t + dt, T)}, device_id_type=MESH)

    def greet(d, _):
        pl.semaphore_signal(barrier, inc=1, device_id={"sp": lax.rem(s + d, S)}, device_id_type=MESH)
        return 0

    lax.fori_loop(1, S, greet, 0)
    tok_buf[t] = tokens[...]
    pl.semaphore_wait(barrier, S + T - 2)

    def tok_copy(dt):
        return pltpu.make_async_remote_copy(
            tokens,
            tok_buf.at[t],
            tok_s.at[dt],
            tok_r.at[dt],
            device_id={"tp": lax.rem(t + dt, T)},
            device_id_type=MESH,
        )

    def tok_in(dt):
        return pltpu.make_async_remote_copy(
            tokens,
            tok_buf.at[lax.rem(t + T - dt, T)],
            tok_s.at[dt],
            tok_r.at[dt],
            device_id={"tp": lax.rem(t + dt, T)},
            device_id_type=MESH,
        )

    for dt in range(1, T):
        tok_copy(dt).start()
    for dt in range(1, T):
        tok_in(dt).wait_recv()

    NB = 32

    def norm_rows(i, _):
        rows = pl.ds(pl.multiple_of(i * NB, NB), NB)
        xs = [tok_buf[k, rows, :].astype(F32) for k in range(T)]
        total = sum(jnp.sum(x * x, axis=-1, keepdims=True) for x in xs)
        r = lax.rsqrt(total * (1.0 / D) + norm_eps)
        for k in range(T):
            cols = slice(k * Dl, (k + 1) * Dl)
            normed[rows, cols] = (xs[k] * r * norm_gain[:, cols]).astype(BF16)
        return 0

    lax.fori_loop(0, R // NB, norm_rows, 0)

    def project(i, store):
        loads[i].wait()
        w = pairs[i][1]
        cols = w.shape[1]
        tile = min(256, cols)
        for c in range(0, cols, tile):
            r = jnp.dot(normed[...], w[:, c : c + tile], preferred_element_type=F32).astype(BF16)
            store(c, tile, r)

    def grouped(write):
        def store(c, tile, r):
            for o in range(0, tile, 2 * HD):
                at = c + o
                write(at // C, at % C, r[:, o : o + 2 * HD])

        return store

    def put_k(gi, col, r):
        kv_send[gi, 0, :, col : col + 2 * HD] = r

    def put_v(gi, col, r):
        kv_send[gi, 1, :, col : col + 2 * HD] = r

    def put_q(gi, col, r):
        q_send[gi, :, col : col + 2 * HD] = r

    def plane(gi, mi):
        return {"sp": gi * M + mi}

    def kv1(dg):
        return pltpu.make_async_remote_copy(
            kv_send.at[lax.rem(g + dg, G)],
            kv_all.at[s],
            kv1_s.at[dg],
            kv_r.at[dg * M],
            device_id=plane(lax.rem(g + dg, G), m),
            device_id_type=MESH,
        )

    def source(dg, dm):
        return lax.rem(g + G - dg, G) * M + lax.rem(m + M - dm, M)

    def kv_in(dg, dm):
        at = kv_all.at[source(dg, dm)]
        return pltpu.make_async_remote_copy(
            at,
            at,
            kv2_s.at[dg * M + dm],
            kv_r.at[dg * M + dm],
            device_id=plane(g, lax.rem(m + 1, M)),
            device_id_type=MESH,
        )

    def kv2(dg, dm):
        at = kv_all.at[source(dg, 0)]
        return pltpu.make_async_remote_copy(
            at,
            at,
            kv2_s.at[dg * M + dm],
            kv_r.at[dg * M + dm],
            device_id=plane(g, lax.rem(m + dm, M)),
            device_id_type=MESH,
        )

    def forward(dg):
        def one(dm, _):
            kv2(dg, dm).start()
            return 0

        lax.fori_loop(1, M, one, 0)

    def q_copy(dg):
        return pltpu.make_async_remote_copy(
            q_send.at[lax.rem(g + dg, G)],
            q_all.at[g],
            q_s.at[dg],
            q_r.at[dg],
            device_id=plane(lax.rem(g + dg, G), m),
            device_id_type=MESH,
        )

    def q_in(dg):
        return pltpu.make_async_remote_copy(
            q_send.at[0],
            q_all.at[lax.rem(g + G - dg, G)],
            q_s.at[dg],
            q_r.at[dg],
            device_id=plane(lax.rem(g + dg, G), m),
            device_id_type=MESH,
        )

    project(0, grouped(put_k))
    project(1, grouped(put_v))
    for dg in range(1, G):
        kv1(dg).start()
    kv_all[s] = kv_send[g]
    forward(0)
    project(2, grouped(put_q))
    for dg in range(1, G):
        q_copy(dg).start()
    q_all[g] = q_send[g]

    def into(ref, first=0):
        def store(c, tile, r):
            ref[first:, c : c + tile] = r

        return store

    project(3, into(band_k, WINDOW))
    project(4, into(band_v, WINDOW))

    def tails():
        nxt = {"sp": lax.rem(s + 1, S)}
        return [
            pltpu.make_async_remote_copy(
                b.at[pl.ds(R, WINDOW)],
                b.at[pl.ds(0, WINDOW)],
                tail_s.at[i],
                tail_r.at[i],
                device_id=nxt,
                device_id_type=MESH,
            )
            for i, b in enumerate((band_k, band_v))
        ]

    @pl.when(s < S - 1)
    def _():
        for cp in tails():
            cp.start()

    @pl.when(s == 0)
    def _():
        band_k[0:WINDOW] = jnp.zeros((WINDOW, band_k.shape[1]), BF16)
        band_v[0:WINDOW] = jnp.zeros((WINDOW, band_v.shape[1]), BF16)

    def relay(dg):
        if dg < G:
            kv_in(dg, 0).wait_recv()
            forward(dg)

    project(5, into(sq_buf))
    project(6, into(sg_buf))
    relay(1)
    project(7, into(pg_buf))
    relay(2)

    @pl.when(s > 0)
    def _():
        for cp in tails():
            cp.wait_recv()

    scale = HD**-0.5
    kv_heads = band_k.shape[1] // HD
    group = sq_buf.shape[1] // band_k.shape[1]
    W = WINDOW
    blocks = R // W
    key_i = lax.broadcasted_iota(jnp.int32, (2 * W, group * W), 0)
    qry_i = lax.rem(lax.broadcasted_iota(jnp.int32, (2 * W, group * W), 1), W)
    lane_head = lax.broadcasted_iota(jnp.int32, (1, group * W), 1) // W
    dist = qry_i - key_i + W
    in_band = (dist >= 0) & (dist < W)

    def window_block(b):
        r0 = b * W
        ok = in_band & (s * R + r0 - W + key_i >= 0)
        for h in range(kv_heads):
            k = band_k[r0 : r0 + 2 * W, h * HD : (h + 1) * HD]
            v = band_v[r0 : r0 + 2 * W, h * HD : (h + 1) * HD]
            q = jnp.concatenate(
                [sq_buf[r0 : r0 + W, (h * group + e) * HD : (h * group + e + 1) * HD] for e in range(group)], axis=0
            )
            sc = jnp.where(ok, dot_nt(k, q) * scale, -jnp.inf)
            sk = jnp.full((1, group * W), sink[0, h * group], F32)
            for e in range(1, group):
                sk = jnp.where(lane_head == e, sink[0, h * group + e], sk)
            top = jnp.maximum(jnp.max(sc, axis=0, keepdims=True), sk)
            w = jnp.exp(sc - top)
            den = jnp.sum(w, axis=0, keepdims=True) + jnp.exp(sk - top)
            probs = (w * (1.0 / den)).astype(BF16)
            o = dot_tn(v, probs)
            o = jnp.concatenate([o[:, e * W : (e + 1) * W] for e in range(group)], axis=0).T
            cols = slice(h * group * HD, (h + 1) * group * HD)
            gate = sg_buf[r0 : r0 + W, cols].astype(F32)
            slide_mix[r0 : r0 + W, cols] = (o * silu(gate)).astype(BF16)

    for b in range(blocks):
        window_block(b)
        if b == 0:
            relay(3)
    for dg in range(4, G):
        relay(dg)

    for dg in range(1, G):
        q_in(dg).wait_recv()
    lane = lax.broadcasted_iota(jnp.int32, (R, 2 * HD), 1)
    for gi in range(G):
        for j in range(Hg):
            q = q_all[gi, :, j * 2 * HD : (j + 1) * 2 * HD].astype(F32) * scale
            q2_buf[gi, j, 0:R, :] = jnp.where(lane < HD, q, 0.0).astype(BF16)
            q2_buf[gi, j, R:, :] = jnp.where(lane < HD, 0.0, q).astype(BF16)
    m_buf[...] = jnp.full(m_buf.shape, -1e30, F32)
    l_buf[...] = jnp.zeros(l_buf.shape, F32)
    acc_buf[...] = jnp.zeros(acc_buf.shape, F32)

    def update(at, gi, masked):
        for j in range(Hg):
            cols = slice(j * 2 * HD, (j + 1) * 2 * HD)
            st = dot_nt(kv_all[at, 0, :, cols], q2_buf[gi, j])
            if masked:
                ki = lax.broadcasted_iota(jnp.int32, (R, 2 * R), 0)
                qi = lax.rem(lax.broadcasted_iota(jnp.int32, (R, 2 * R), 1), R)
                st = jnp.where(qi >= ki, st, -jnp.inf)
            old = m_buf[gi, j]
            new = jnp.maximum(old, jnp.max(st, axis=0, keepdims=True))
            f = jnp.exp(old - new)
            p = jnp.exp(st - new)
            m_buf[gi, j] = new
            l_buf[gi, j] = l_buf[gi, j] * f + jnp.sum(p, axis=0, keepdims=True)
            acc_buf[gi, j] = acc_buf[gi, j] * f + dot_tn(kv_all[at, 1, :, cols], p.astype(BF16))

    def process(at):
        def one(gi, _):
            mine = gi * M + m

            @pl.when(at < mine)
            def _():
                update(at, gi, False)

            @pl.when(at == mine)
            def _():
                update(at, gi, True)

            return 0

        lax.fori_loop(0, G, one, 0)

    def near(dg, _):
        process(source(dg, 0))
        return 0

    lax.fori_loop(0, G, near, 0)

    def far(i, _):
        dg = i // (M - 1)
        dm = 1 + lax.rem(i, M - 1)
        kv_in(dg, dm).wait_recv()
        process(source(dg, dm))
        return 0

    if M > 1:
        lax.fori_loop(0, G * (M - 1), far, 0)

    def ret_copy(dg):
        return pltpu.make_async_remote_copy(
            ret_send.at[lax.rem(g + dg, G)],
            ret_all.at[g],
            ret_s.at[dg],
            ret_r.at[dg],
            device_id=plane(lax.rem(g + dg, G), m),
            device_id_type=MESH,
        )

    def ret_in(dg):
        return pltpu.make_async_remote_copy(
            ret_send.at[0],
            ret_all.at[lax.rem(g + G - dg, G)],
            ret_s.at[dg],
            ret_r.at[dg],
            device_id=plane(lax.rem(g + dg, G), m),
            device_id_type=MESH,
        )

    def finish(gi):
        for j in range(Hg):
            a = acc_buf[gi, j] * (1.0 / l_buf[gi, j])
            d = a[:, 0:R] - lam[0, g * Hg + j] * a[:, R:]
            sq = jnp.mean(d * d, axis=0, keepdims=True)
            y = (d * (lax.rsqrt(sq + norm_eps) * head_scale)).T * head_gain[...]
            ret_send[gi, :, j * 2 * HD : (j + 1) * 2 * HD] = y.astype(BF16)

    for dg in range(1, G):
        finish(lax.rem(g + dg, G))
        ret_copy(dg).start()
    finish(g)
    ret_all[g] = ret_send[g]

    loads[8].wait()
    NT = min(512, D)
    for c in range(0, D, NT):
        part[:, c : c + NT] = jnp.dot(slide_mix[...], wo[:, c : c + NT], preferred_element_type=F32)
    for dg in range(1, G):
        ret_in(dg).wait_recv()
    for gi in range(G):
        gate = pg_buf[:, gi * C : (gi + 1) * C].astype(F32)
        paired_mix[:, gi * C : (gi + 1) * C] = (ret_all[gi].astype(F32) * silu(gate)).astype(BF16)
    loads[9].wait()
    Rt = R // T
    for c in range(0, D, NT):
        r = part[:, c : c + NT] + jnp.dot(paired_mix[...], po[:, c : c + NT], preferred_element_type=F32)
        r = r.astype(BF16)
        for k in range(T):
            part_bf[k, :, c : c + NT] = r[k * Rt : (k + 1) * Rt]

    def rs_copy(dt):
        return pltpu.make_async_remote_copy(
            part_bf.at[lax.rem(t + dt, T)],
            rs_buf.at[dt],
            rs_s.at[dt],
            rs_r.at[dt],
            device_id={"tp": lax.rem(t + dt, T)},
            device_id_type=MESH,
        )

    for dt in range(1, T):
        rs_copy(dt).start()
    for dt in range(1, T):
        rs_copy(dt).wait_recv()
    for c in range(0, D, NT):
        total = part_bf[t, :, c : c + NT].astype(F32)
        for dt in range(1, T):
            total = total + rs_buf[dt, :, c : c + NT].astype(F32)
        out[:, c : c + NT] = total.astype(BF16)

    for dt in range(1, T):
        tok_copy(dt).wait_send()
        rs_copy(dt).wait_send()
    for dg in range(1, G):
        kv1(dg).wait_send()
        q_copy(dg).wait_send()
        ret_copy(dg).wait_send()

    def drain(i, _):
        kv2(i // (M - 1), 1 + lax.rem(i, M - 1)).wait_send()
        return 0

    if M > 1:
        lax.fori_loop(0, G * (M - 1), drain, 0)

    @pl.when(s < S - 1)
    def _():
        for cp in tails():
            cp.wait_send()


def per_device(S, T, tokens, norm_gain, wq, wk, wv, wg, sink, pq, pk, pv, pg, lam, head_gain, wo, po):
    R, Dl = tokens.shape
    D = Dl * T
    A = wq.shape[1]
    KC = wk.shape[1]
    B = pq.shape[1]
    H = B // (2 * HD)
    G = math.gcd(H, S)
    Hg = H // G
    C = Hg * 2 * HD
    vmem = pl.BlockSpec(memory_space=pltpu.VMEM)
    smem = pl.BlockSpec(memory_space=pltpu.SMEM)
    hbm = pl.BlockSpec(memory_space=pl.ANY)
    dma = pltpu.SemaphoreType.DMA
    V = pltpu.VMEM
    scratch = [V(w.shape, BF16) for w in (wq, wk, wv, wg, pq, pk, pv, pg, wo, po)]
    scratch += [
        V((T, R, Dl), BF16),
        V((R, D), BF16),
        V((WINDOW + R, KC), BF16),
        V((WINDOW + R, KC), BF16),
        V((R, A), BF16),
        V((R, A), BF16),
        V((R, B), BF16),
        V((R, A), BF16),
        V((R, B), BF16),
        V((G, 2, R, C), BF16),
        V((G, R, C), BF16),
        V((S, 2, R, C), BF16),
        V((G, R, C), BF16),
        V((G, Hg, 2 * R, 2 * HD), BF16),
        V((G, Hg, 1, 2 * R), F32),
        V((G, Hg, 1, 2 * R), F32),
        V((G, Hg, 2 * HD, 2 * R), F32),
        V((G, R, C), BF16),
        V((G, R, C), BF16),
        V((R, D), F32),
        V((T, R // T, D), BF16),
        V((T, R // T, D), BF16),
        dma((10,)),
        dma((T,)),
        dma((T,)),
        dma((G,)),
        dma((S,)),
        dma((S,)),
        dma((G,)),
        dma((G,)),
        dma((2,)),
        dma((2,)),
        dma((G,)),
        dma((G,)),
        dma((T,)),
        dma((T,)),
    ]
    return pl.pallas_call(
        functools.partial(kernel, S, T),
        out_shape=jax.ShapeDtypeStruct((R // T, D), BF16),
        in_specs=[vmem, vmem, hbm, hbm, hbm, hbm, smem, hbm, hbm, hbm, hbm, smem, vmem, hbm, hbm],
        out_specs=vmem,
        scratch_shapes=scratch,
        compiler_params=pltpu.CompilerParams(
            collective_id=0, has_side_effects=True, vmem_limit_bytes=60 * 1024 * 1024
        ),
        name="layer",
    )(
        tokens,
        norm_gain.reshape(1, D),
        wq,
        wk,
        wv,
        wg,
        sink.reshape(1, -1),
        pq,
        pk,
        pv,
        pg,
        lam.reshape(1, -1),
        head_gain.reshape(1, -1),
        wo,
        po,
    )


def solution(mesh):
    S, T = mesh.shape["sp"], mesh.shape["tp"]
    in_specs = (
        P("sp", "tp"),
        P(),
        P(None, "tp"),
        P(None, "tp"),
        P(None, "tp"),
        P(None, "tp"),
        P("tp"),
        P(None, "tp"),
        P(None, "tp"),
        P(None, "tp"),
        P(None, "tp"),
        P("tp"),
        P(),
        P("tp", None),
        P("tp", None),
    )
    return jax.shard_map(
        functools.partial(per_device, S, T),
        mesh=mesh,
        in_specs=in_specs,
        out_specs=P(("sp", "tp"), None),
        check_vma=False,
    )
```

time: 271 us -> 62.8 us (0.23)
  the two profiles are of different devices: /device:TPU:31 before, /device:TPU:1 now
where the time goes in v1:
time: 62.8 us; the launch traced here: 62.6 us
  Pallas kernels  60.7 us (97%)
  local copies, waits for them, and re-layouts  1.88 us (3%)
    pallas_call x1, Pallas kernels, per_device(): pl.pallas_call(functools.partial(kernel, S, T), out_shape=jax.ShapeDtypeS...  60.7 us
    unnamed x1, local copies, waits for them, and re-layouts  1.88 us

profile of v1, /device:TPU:1, one launch (start us, length us, event | category | flops | bytes accessed | tf_op | source)
XLA Modules:
  0.0 62.6 jit_solution(3357907254646732609)
XLA Ops:
  0.0 60.7 %layer.1 = bf16[128,2048]{1,0:T(8,128)(2,1)} custom-call(bf16[256,1024]{1,0:T(8,128)(2,1)} %tokens.1, f32[1,2048]{1,0:T(1,128)} %bitcast.4, bf16[2048,512]{1,0:T(8,128)(2,1)} %wq_h.1, bf16[2048,256]{1,0:T(8,128)(2,1)} %wk_h.1, bf16[2048,256]{1,0:T(8,128)(2,1)} %wv_h.1, bf16[2048,512]{1,0:T(8,128)(2,1)} %wg_h.1, f32[1,8]{1,0:T(1,128)} %bitcast.5, ...), custom_call_target="tpu_custom_call" | custom-call | tf_op jit(solution)/shard_map/layer/pallas_call | solution.py:566
  60.7 1.9 %copy.17 = bf16[128,2048]{1,0:T(8,128)(2,1)} copy(bf16[128,2048]{1,0:T(8,128)(2,1)} %layer.1) | data formatting | bytes 1048576

commit v2 on v1

--- a/solution.py
+++ b/solution.py
@@ -81,7 +81,6 @@
     ret_all,
     part,
     part_bf,
-    rs_buf,
     w_sem,
     tok_s,
     tok_r,
@@ -109,7 +108,7 @@
     g = s // M
     m = lax.rem(s, M)
 
-    pairs = [(pk_h, pk), (pv_h, pv), (pq_h, pq), (wk_h, wk), (wv_h, wv), (wq_h, wq), (wg_h, wg), (pg_h, pg), (wo_h, wo), (po_h, po)]
+    pairs = [(pq_h, pq), (pk_h, pk), (pv_h, pv), (wk_h, wk), (wv_h, wv), (wq_h, wq), (wg_h, wg), (pg_h, pg), (wo_h, wo), (po_h, po)]
     loads = [pltpu.make_async_copy(a, b, w_sem.at[i]) for i, (a, b) in enumerate(pairs)]
     for cp in loads:
         cp.start()
@@ -126,30 +125,32 @@
     tok_buf[t] = tokens[...]
     pl.semaphore_wait(barrier, S + T - 2)
 
-    def tok_copy(dt):
-        return pltpu.make_async_remote_copy(
-            tokens,
-            tok_buf.at[t],
-            tok_s.at[dt],
-            tok_r.at[dt],
+    TC = tok_s.shape[1]
+    CR = R // TC
+
+    def tok_copy(dt, i):
+        return pltpu.make_async_remote_copy(
+            tokens.at[pl.ds(i * CR, CR)],
+            tok_buf.at[t, pl.ds(i * CR, CR)],
+            tok_s.at[dt, i],
+            tok_r.at[dt, i],
             device_id={"tp": lax.rem(t + dt, T)},
             device_id_type=MESH,
         )
 
-    def tok_in(dt):
-        return pltpu.make_async_remote_copy(
-            tokens,
-            tok_buf.at[lax.rem(t + T - dt, T)],
-            tok_s.at[dt],
-            tok_r.at[dt],
+    def tok_in(dt, i):
+        return pltpu.make_async_remote_copy(
+            tokens.at[pl.ds(i * CR, CR)],
+            tok_buf.at[lax.rem(t + T - dt, T), pl.ds(i * CR, CR)],
+            tok_s.at[dt, i],
+            tok_r.at[dt, i],
             device_id={"tp": lax.rem(t + dt, T)},
             device_id_type=MESH,
         )
 
-    for dt in range(1, T):
-        tok_copy(dt).start()
-    for dt in range(1, T):
-        tok_in(dt).wait_recv()
+    for i in range(TC):
+        for dt in range(1, T):
+            tok_copy(dt, i).start()
 
     NB = 32
 
@@ -163,7 +164,10 @@
             normed[rows, cols] = (xs[k] * r * norm_gain[:, cols]).astype(BF16)
         return 0
 
-    lax.fori_loop(0, R // NB, norm_rows, 0)
+    for i in range(TC):
+        for dt in range(1, T):
+            tok_in(dt, i).wait_recv()
+        lax.fori_loop(i * CR // NB, (i + 1) * CR // NB, norm_rows, 0)
 
     def project(i, store):
         loads[i].wait()
@@ -256,16 +260,16 @@
             device_id_type=MESH,
         )
 
-    project(0, grouped(put_k))
-    project(1, grouped(put_v))
+    project(0, grouped(put_q))
+    for dg in range(1, G):
+        q_copy(dg).start()
+    q_all[g] = q_send[g]
+    project(1, grouped(put_k))
+    project(2, grouped(put_v))
     for dg in range(1, G):
         kv1(dg).start()
     kv_all[s] = kv_send[g]
     forward(0)
-    project(2, grouped(put_q))
-    for dg in range(1, G):
-        q_copy(dg).start()
-    q_all[g] = q_send[g]
 
     def into(ref, first=0):
         def store(c, tile, r):
@@ -301,15 +305,12 @@
         band_v[0:WINDOW] = jnp.zeros((WINDOW, band_v.shape[1]), BF16)
 
     def relay(dg):
-        if dg < G:
-            kv_in(dg, 0).wait_recv()
-            forward(dg)
+        kv_in(dg, 0).wait_recv()
+        forward(dg)
 
     project(5, into(sq_buf))
     project(6, into(sg_buf))
-    relay(1)
     project(7, into(pg_buf))
-    relay(2)
 
     @pl.when(s > 0)
     def _():
@@ -352,10 +353,8 @@
 
     for b in range(blocks):
         window_block(b)
-        if b == 0:
-            relay(3)
-    for dg in range(4, G):
-        relay(dg)
+    if G > 1:
+        relay(1)
 
     for dg in range(1, G):
         q_in(dg).wait_recv()
@@ -401,22 +400,6 @@
 
         lax.fori_loop(0, G, one, 0)
 
-    def near(dg, _):
-        process(source(dg, 0))
-        return 0
-
-    lax.fori_loop(0, G, near, 0)
-
-    def far(i, _):
-        dg = i // (M - 1)
-        dm = 1 + lax.rem(i, M - 1)
-        kv_in(dg, dm).wait_recv()
-        process(source(dg, dm))
-        return 0
-
-    if M > 1:
-        lax.fori_loop(0, G * (M - 1), far, 0)
-
     def ret_copy(dg):
         return pltpu.make_async_remote_copy(
             ret_send.at[lax.rem(g + dg, G)],
@@ -445,10 +428,39 @@
             y = (d * (lax.rsqrt(sq + norm_eps) * head_scale)).T * head_gain[...]
             ret_send[gi, :, j * 2 * HD : (j + 1) * 2 * HD] = y.astype(BF16)
 
-    for dg in range(1, G):
-        finish(lax.rem(g + dg, G))
-        ret_copy(dg).start()
-    finish(g)
+    def step(dg, _):
+        def far(dm, _):
+            kv_in(dg, dm).wait_recv()
+            process(source(dg, dm))
+            return 0
+
+        half = max(1, M // 2)
+        process(source(dg, 0))
+        lax.fori_loop(1, half, far, 0)
+
+        @pl.when(dg + 2 < G)
+        def _():
+            relay(dg + 2)
+
+        lax.fori_loop(half, M, far, 0)
+
+        def close(gi, last):
+            last = jnp.maximum(last, lax.rem(g + G - gi, G))
+
+            @pl.when(last == dg)
+            def _():
+                finish(gi)
+
+                @pl.when(gi != g)
+                def _():
+                    ret_copy(lax.rem(gi + G - g, G)).start()
+
+            return last
+
+        lax.fori_loop(0, G, close, 0)
+        return 0
+
+    lax.fori_loop(0, G, step, 0)
     ret_all[g] = ret_send[g]
 
     loads[8].wait()
@@ -462,35 +474,33 @@
         paired_mix[:, gi * C : (gi + 1) * C] = (ret_all[gi].astype(F32) * silu(gate)).astype(BF16)
     loads[9].wait()
     Rt = R // T
+
+    def rs_copy(dt, i):
+        cols = pl.ds(i * NT, NT)
+        return pltpu.make_async_remote_copy(
+            part_bf.at[lax.rem(t + dt, T), :, cols],
+            out.at[dt, :, cols],
+            rs_s.at[dt, i],
+            rs_r.at[dt, i],
+            device_id={"tp": lax.rem(t + dt, T)},
+            device_id_type=MESH,
+        )
+
     for c in range(0, D, NT):
         r = part[:, c : c + NT] + jnp.dot(paired_mix[...], po[:, c : c + NT], preferred_element_type=F32)
         r = r.astype(BF16)
         for k in range(T):
             part_bf[k, :, c : c + NT] = r[k * Rt : (k + 1) * Rt]
-
-    def rs_copy(dt):
-        return pltpu.make_async_remote_copy(
-            part_bf.at[lax.rem(t + dt, T)],
-            rs_buf.at[dt],
-            rs_s.at[dt],
-            rs_r.at[dt],
-            device_id={"tp": lax.rem(t + dt, T)},
-            device_id_type=MESH,
-        )
+        for dt in range(1, T):
+            rs_copy(dt, c // NT).start()
+    out[0] = part_bf[t]
+    for c in range(0, D, NT):
+        for dt in range(1, T):
+            rs_copy(dt, c // NT).wait()
 
     for dt in range(1, T):
-        rs_copy(dt).start()
-    for dt in range(1, T):
-        rs_copy(dt).wait_recv()
-    for c in range(0, D, NT):
-        total = part_bf[t, :, c : c + NT].astype(F32)
-        for dt in range(1, T):
-            total = total + rs_buf[dt, :, c : c + NT].astype(F32)
-        out[:, c : c + NT] = total.astype(BF16)
-
-    for dt in range(1, T):
-        tok_copy(dt).wait_send()
-        rs_copy(dt).wait_send()
+        for i in range(TC):
+            tok_copy(dt, i).wait_send()
     for dg in range(1, G):
         kv1(dg).wait_send()
         q_copy(dg).wait_send()
@@ -547,10 +557,9 @@
         V((G, R, C), BF16),
         V((R, D), F32),
         V((T, R // T, D), BF16),
-        V((T, R // T, D), BF16),
         dma((10,)),
-        dma((T,)),
-        dma((T,)),
+        dma((T, 4)),
+        dma((T, 4)),
         dma((G,)),
         dma((S,)),
         dma((S,)),
@@ -560,12 +569,12 @@
         dma((2,)),
         dma((G,)),
         dma((G,)),
-        dma((T,)),
-        dma((T,)),
+        dma((T, max(1, D // 512))),
+        dma((T, max(1, D // 512))),
     ]
-    return pl.pallas_call(
+    shares = pl.pallas_call(
         functools.partial(kernel, S, T),
-        out_shape=jax.ShapeDtypeStruct((R // T, D), BF16),
+        out_shape=jax.ShapeDtypeStruct((T, R // T, D), BF16),
         in_specs=[vmem, vmem, hbm, hbm, hbm, hbm, smem, hbm, hbm, hbm, hbm, smem, vmem, hbm, hbm],
         out_specs=vmem,
         scratch_shapes=scratch,
@@ -590,6 +599,7 @@
         wo,
         po,
     )
+    return jnp.sum(shares.astype(F32), axis=0).astype(BF16)
 
 
 def solution(mesh):

time: 62.8 us -> 63 us (level)
  the two profiles are of different devices: /device:TPU:1 before, /device:TPU:31 now
where the time goes in v2:
time: 63 us; the launch traced here: 62.8 us
  Pallas kernels  60.4 us (96%)
  other arithmetic  2.36 us (4%)
    pallas_call x1, Pallas kernels, per_device(): pl.pallas_call(functools.partial(kernel, S, T), out_shape=jax.ShapeDtypeS...  60.4 us
    reduce_sum x1, other arithmetic, per_device(): return jnp.sum(shares.astype(F32), axis=0).astype(BF16)  2.36 us

profile of v2, /device:TPU:31, one launch (start us, length us, event | category | flops | bytes accessed | tf_op | source)
XLA Modules:
  0.0 62.8 jit_solution(10682800341923887891)
XLA Ops:
  0.0 60.4 %layer.1 = bf16[2,128,2048]{2,1,0:T(8,128)(2,1)} custom-call(bf16[256,1024]{1,0:T(8,128)(2,1)} %tokens.1, f32[1,2048]{1,0:T(1,128)} %bitcast.4, bf16[2048,512]{1,0:T(8,128)(2,1)} %wq_h.1, bf16[2048,256]{1,0:T(8,128)(2,1)} %wk_h.1, bf16[2048,256]{1,0:T(8,128)(2,1)} %wv_h.1, bf16[2048,512]{1,0:T(8,128)(2,1)} %wg_h.1, f32[1,8]{1,0:T(1,128)} %bitcast.5, ...), custom_call_target="tpu_custom_call" | custom-call | tf_op jit(solution)/shard_map/layer/pallas_call | solution.py:575
  60.4 2.4 %reduce_sum.12 = bf16[128,2048]{1,0:T(8,128)(2,1)} reduce(bf16[2,128,2048]{2,1,0:T(8,128)(2,1)} %layer.1, bf16[]{:T(256)} %constant.2.clone.1), dimensions={0}, to_apply=%region_0.0 | reduce | flops 262144 | bytes 1572866 | tf_op jit(solution)/shard_map/reduce_sum | solution.py:602

commit v3 on v2

--- a/solution.py
+++ b/solution.py
@@ -260,16 +260,16 @@
             device_id_type=MESH,
         )
 
-    project(0, grouped(put_q))
-    for dg in range(1, G):
-        q_copy(dg).start()
-    q_all[g] = q_send[g]
     project(1, grouped(put_k))
     project(2, grouped(put_v))
     for dg in range(1, G):
         kv1(dg).start()
     kv_all[s] = kv_send[g]
     forward(0)
+    project(0, grouped(put_q))
+    for dg in range(1, G):
+        q_copy(dg).start()
+    q_all[g] = q_send[g]
 
     def into(ref, first=0):
         def store(c, tile, r):

time: 63 us -> 64 us (1.016)
  Pallas kernels: 60.4 us -> 61.5 us
    pallas_call x1, Pallas kernels: 60.4 us -> 61.5 us  [per_device(): pl.pallas_call(functools.partial(kernel, S, T), out_shape=jax.ShapeDtypeS...]
where the time goes in v3:
time: 64 us; the launch traced here: 63.9 us
  Pallas kernels  61.5 us (96%)
  other arithmetic  2.36 us (4%)
    pallas_call x1, Pallas kernels, per_device(): pl.pallas_call(functools.partial(kernel, S, T), out_shape=jax.ShapeDtypeS...  61.5 us
    reduce_sum x1, other arithmetic, per_device(): return jnp.sum(shares.astype(F32), axis=0).astype(BF16)  2.36 us

profile of v3, /device:TPU:31, one launch (start us, length us, event | category | flops | bytes accessed | tf_op | source)
XLA Modules:
  0.0 63.9 jit_solution(12766408604819636242)
XLA Ops:
  0.0 61.5 %layer.1 = bf16[2,128,2048]{2,1,0:T(8,128)(2,1)} custom-call(bf16[256,1024]{1,0:T(8,128)(2,1)} %tokens.1, f32[1,2048]{1,0:T(1,128)} %bitcast.4, bf16[2048,512]{1,0:T(8,128)(2,1)} %wq_h.1, bf16[2048,256]{1,0:T(8,128)(2,1)} %wk_h.1, bf16[2048,256]{1,0:T(8,128)(2,1)} %wv_h.1, bf16[2048,512]{1,0:T(8,128)(2,1)} %wg_h.1, f32[1,8]{1,0:T(1,128)} %bitcast.5, ...), custom_call_target="tpu_custom_call" | custom-call | tf_op jit(solution)/shard_map/layer/pallas_call | solution.py:575
  61.5 2.4 %reduce_sum.12 = bf16[128,2048]{1,0:T(8,128)(2,1)} reduce(bf16[2,128,2048]{2,1,0:T(8,128)(2,1)} %layer.1, bf16[]{:T(256)} %constant.2.clone.1), dimensions={0}, to_apply=%region_0.0 | reduce | flops 262144 | bytes 1572866 | tf_op jit(solution)/shard_map/reduce_sum | solution.py:602
